TPU v7x, 32 devices: a whole 2x2x4 slice. The times are simulated.
32 devices in a mesh: sp: 8 (over z, x), tp: 4 (over y, core).
Axes of the slice: x: 2, y: 2, z: 4, core: 2. Of those that a mesh axis runs over, the one named last changes fastest.
Arguments:
- sequence_embeddings: bfloat16 [3072, 2048], P('sp'), may hold values from -6 to 6
- entry_rescale_vector: bfloat16 [2048], replicated, may hold values from 0.099609375 to 1.8984375
- probe_matrix: bfloat16 [2048, 1024], P('sp', 'tp'), may hold values from -0.125 to 0.125
- onward_retain_matrix: bfloat16 [2048, 1024], P('sp', 'tp'), may hold values from -0.125 to 0.125
- reverse_retain_matrix: bfloat16 [2048, 1024], P('sp', 'tp'), may hold values from -0.125 to 0.125
- content_matrix: bfloat16 [2048, 1024], P('sp', 'tp'), may hold values from -0.125 to 0.125
- emission_switch_matrix: bfloat16 [2048, 1024], P('sp', 'tp'), may hold values from -0.125 to 0.125
- pointwise_content_matrix: bfloat16 [2048, 1024], P('sp', 'tp'), may hold values from -0.125 to 0.125
- pointwise_switch_matrix: bfloat16 [2048, 1024], P('sp', 'tp'), may hold values from -0.125 to 0.125
- retain_lower_slack: float32 [2, 1024], P(None, 'tp'), may hold values from 0 to 0.034, as said below
- extra_log_shrink: float32 [2, 3072, 8], P(None, 'sp', 'tp'), may hold values from -1 to 0
- subspace_rescale: bfloat16 [128], replicated, may hold values from 0.099609375 to 1.8984375
- filter_kernel_coefs: bfloat16 [31, 1024], P(None, 'tp'), may hold values from -1 to 1
- channel_cluster_scale: bfloat16 [1024], P('tp'), may hold values from 0.099609375 to 1.8984375
- scan_readout_matrix: bfloat16 [1024, 2048], P('tp', 'sp'), may hold values from -0.125 to 0.125
- filter_readout_matrix: bfloat16 [1024, 2048], P('tp', 'sp'), may hold values from -0.125 to 0.125
Outputs:
- mixed: bfloat16 [3072, 2048], P(('sp', 'tp'))
Inputs may be any that keep to these rules, and one draw needn't show every extreme that they name: `retain_lower_slack`: every entry is positive.
All inputs are finite; a program needn't handle non-finite values.
Results may differ from a plain program's by a relative error of at most 0.015.
Values may be sent and summed in bfloat16 or wider, within the bound.
A program may use at most 64 MiB of HBM per device.

v0:
```python
import jax
import jax.numpy as jnp
from jax import lax
from jax.sharding import PartitionSpec as P

KEY_DIM = 128
VALUE_DIM = 128
GROUP_CH = 128
CONV_KW = 31
BLOCK = 64


precise_setting = lax.Precision.HIGHEST


def prefix(array, axis, join, neutral, backward):
    count = lax.axis_size(axis)
    place = lax.axis_index(axis)
    ahead = count - 1 - place if backward else place
    gathered = jax.tree.map(
        lambda a, kind: lax.all_gather(a.astype(kind), axis),
        array,
        jax.tree.map(lambda a: jnp.bfloat16 if a.dtype == jnp.float32 else a.dtype, array),
    )
    state = jax.tree.map(lambda a, e: jnp.zeros_like(a) + jnp.asarray(e, a.dtype), array, neutral)

    def one(turn, state):
        source = count - 1 - turn if backward else turn
        return join(
            state,
            jax.tree.map(
                lambda a, own: lax.dynamic_index_in_dim(a, source, 0, False).astype(own.dtype),
                gathered,
                array,
            ),
        )

    return lax.fori_loop(0, ahead, one, state)


def extended(block, sides, width):
    for axis, dim in sides:
        count = lax.axis_size(axis)
        forward = [(i, i + 1) for i in range(count - 1)]
        backward = [(target, source) for source, target in forward]
        low = lax.ppermute(
            lax.slice_in_dim(block, block.shape[dim] - width, None, axis=dim), axis, forward
        )
        high = lax.ppermute(lax.slice_in_dim(block, 0, width, axis=dim), axis, backward)
        block = jnp.concatenate([low, block, high], axis=dim)
    return block


def normalize(sequence_embeddings, entry_rescale_vector):
    floats = sequence_embeddings.astype(jnp.float32)
    factor = lax.rsqrt(jnp.mean(floats * floats, axis=-1, keepdims=True) + 1e-06)
    return (floats * factor * entry_rescale_vector.astype(jnp.float32)).astype(jnp.bfloat16)


def sigmoid_switch_entries(
    emission_switch_scores, retain_lower_slack_line, drawn_extra_lines, subspace_amount
):
    length = emission_switch_scores.shape[0]
    retain_slack_amount = retain_lower_slack_line[None, :] * jax.nn.sigmoid(-emission_switch_scores)
    retain_slack_amount = retain_slack_amount.reshape(length, subspace_amount, -1)
    log_shrink_amount = jnp.log1p(-retain_slack_amount) + drawn_extra_lines[:, :, None]
    return (log_shrink_amount, retain_slack_amount)


def block_recurrence(queries, log_shrink_amount, retain_slack_amount, value_rows, initial):
    length, subspace_amount, key_dim = queries.shape
    block_count = length // BLOCK

    def to_blocks(tensor):
        return tensor.reshape(block_count, BLOCK, subspace_amount, tensor.shape[-1])

    lower_mask = jnp.tril(jnp.ones((BLOCK, BLOCK), jnp.float32))

    def advance(state_carried_over, blocked):
        query_block, decay_block, gap_block, value_block_rows = blocked
        running_state = jnp.cumsum(decay_block, axis=0)
        block_grand_total = running_state[-1]
        lifted_values = query_block * jnp.exp(running_state)
        lowered = gap_block * jnp.exp(-running_state)
        scores = (
            jnp.einsum("thk,shk->hts", lifted_values, lowered, precision=precise_setting)
            * lower_mask
        )
        within_block = jnp.einsum(
            "hts,shv->thv", scores, value_block_rows, precision=precise_setting
        )
        output_rows = within_block + jnp.einsum(
            "ipm,pmo->ipo", lifted_values, state_carried_over, precision=precise_setting
        )
        fading_factor = gap_block * jnp.exp(block_grand_total - running_state)
        updated_state = jnp.exp(block_grand_total)[:, :, None] * state_carried_over + jnp.einsum(
            "fwd,fwt->wdt", fading_factor, value_block_rows, precision=precise_setting
        )
        return (updated_state, output_rows)

    last_state, output_rows = lax.scan(
        advance,
        initial,
        (
            to_blocks(queries),
            to_blocks(log_shrink_amount),
            to_blocks(retain_slack_amount),
            to_blocks(value_rows),
        ),
    )
    return (output_rows.reshape(length, subspace_amount, value_rows.shape[-1]), last_state)


def running_log(log_shrink_amount):
    length, subspace_amount, key_dim = log_shrink_amount.shape
    blocks = log_shrink_amount.reshape(length // BLOCK, BLOCK, subspace_amount, key_dim)
    inside = jnp.cumsum(blocks, axis=1)
    offsets = jnp.cumsum(inside[:, -1], axis=0) - inside[:, -1]
    return (inside + offsets[:, None]).reshape(length, subspace_amount, key_dim)


def join_segments(earlier, later):
    return (earlier[0] + later[0], jnp.exp(later[0])[:, :, None] * earlier[1] + later[1])


def exchange_states(summary, reverse):
    identity = (jnp.zeros_like(summary[0]), jnp.zeros_like(summary[1]))
    if reverse:
        return prefix(summary, "sp", join_segments, identity, True)
    return prefix(summary, "sp", join_segments, identity, False)


def mix_direction(queries, log_shrink_amount, retain_slack_amount, value_rows, reverse):
    if reverse:
        queries, log_shrink_amount, retain_slack_amount, value_rows = (
            jnp.flip(tensor, 0)
            for tensor in (queries, log_shrink_amount, retain_slack_amount, value_rows)
        )
    running_state = running_log(log_shrink_amount)
    local_end = jnp.einsum(
        "opl,ops->pls",
        retain_slack_amount * jnp.exp(running_state[-1] - running_state),
        value_rows,
        precision=precise_setting,
    )
    incoming = exchange_states((running_state[-1], local_end), reverse)[1]
    output_rows = block_recurrence(
        queries, log_shrink_amount, retain_slack_amount, value_rows, incoming
    )[0]
    if reverse:
        output_rows = jnp.flip(output_rows, 0)
    return output_rows


def readout(summed, subspace_rescale, out_gate):
    length = summed.shape[0]
    factor = lax.rsqrt(jnp.mean(summed * summed, axis=-1, keepdims=True) + 1e-06)
    scaled = summed * factor * subspace_rescale.astype(jnp.float32)
    return (scaled.reshape(length, -1) * jax.nn.silu(out_gate)).astype(jnp.bfloat16)


def depthwise(framed, filter_kernel_coefs):
    channels = framed.shape[1]
    result = lax.conv_general_dilated(
        framed[None],
        filter_kernel_coefs[:, None, :],
        (1,),
        "VALID",
        dimension_numbers=("NWC", "WIO", "NWC"),
        feature_group_count=channels,
        preferred_element_type=jnp.float32,
    )
    return result[0]


def group_norm_silu(conv_sum, channel_cluster_scale):
    length, channels = conv_sum.shape
    grouped = conv_sum.reshape(length, -1, GROUP_CH)
    centred = grouped - jnp.mean(grouped, axis=-1, keepdims=True)
    variance = jnp.mean(centred * centred, axis=-1, keepdims=True)
    standard = (centred * lax.rsqrt(variance + 1e-05)).reshape(length, channels)
    return jax.nn.silu(standard * channel_cluster_scale.astype(jnp.float32)).astype(jnp.bfloat16)


def on_device(
    sequence_embeddings,
    entry_rescale_vector,
    probe_matrix,
    onward_retain_matrix,
    reverse_retain_matrix,
    content_matrix,
    emission_switch_matrix,
    pointwise_content_matrix,
    pointwise_switch_matrix,
    retain_lower_slack,
    extra_log_shrink,
    subspace_rescale,
    filter_kernel_coefs,
    channel_cluster_scale,
    scan_readout_matrix,
    filter_readout_matrix,
):
    normed = normalize(sequence_embeddings, entry_rescale_vector)
    length = sequence_embeddings.shape[0]
    weights = (
        probe_matrix,
        onward_retain_matrix,
        reverse_retain_matrix,
        content_matrix,
        emission_switch_matrix,
        pointwise_content_matrix,
        pointwise_switch_matrix,
    )
    pieces = (
        lax.all_gather(weights[0], "sp", axis=0, tiled=True),
        lax.all_gather(weights[1], "sp", axis=0, tiled=True),
        lax.all_gather(weights[2], "sp", axis=0, tiled=True),
        lax.all_gather(weights[3], "sp", axis=0, tiled=True),
        lax.all_gather(weights[4], "sp", axis=0, tiled=True),
        lax.all_gather(weights[5], "sp", axis=0, tiled=True),
        lax.all_gather(weights[6], "sp", axis=0, tiled=True),
    )
    projected = tuple(
        (
            jnp.dot(normed, weight_piece, preferred_element_type=jnp.float32)
            for weight_piece in pieces
        )
    )
    (
        pre_query,
        onward_retain_scores,
        reverse_retain_scores,
        pre_value,
        emission_switch_scores,
        pre_glu_a,
        pre_glu_b,
    ) = projected
    glu = (pre_glu_a * jax.nn.sigmoid(pre_glu_b)).astype(jnp.bfloat16)
    framed = extended(glu, (("sp", 0),), CONV_KW // 2)
    conv_out = group_norm_silu(depthwise(framed, filter_kernel_coefs), channel_cluster_scale)
    subspace_amount = pre_query.shape[1] // KEY_DIM
    queries = jax.nn.silu(pre_query).reshape(length, subspace_amount, KEY_DIM)
    value_rows = pre_value.reshape(length, subspace_amount, VALUE_DIM)
    onward_shrink_multiplier, onward_retain_slack = sigmoid_switch_entries(
        onward_retain_scores, retain_lower_slack[0], extra_log_shrink[0], subspace_amount
    )
    reverse_shrink_multiplier, reverse_retain_slack = sigmoid_switch_entries(
        reverse_retain_scores, retain_lower_slack[1], extra_log_shrink[1], subspace_amount
    )
    forward_out = mix_direction(
        queries, onward_shrink_multiplier, onward_retain_slack, value_rows, False
    )
    backward_out = mix_direction(
        queries, reverse_shrink_multiplier, reverse_retain_slack, value_rows, True
    )
    rec_out = readout(forward_out + backward_out, subspace_rescale, emission_switch_scores)
    slabs = (
        lax.all_gather(scan_readout_matrix, "tp", axis=0, tiled=True),
        lax.all_gather(filter_readout_matrix, "tp", axis=0, tiled=True),
    )
    rec_width = slabs[0].shape[0]
    stacked = jnp.concatenate(slabs, axis=0)
    rec_rows, conv_rows = (
        lax.all_to_all(rec_out, "tp", split_axis=0, concat_axis=1, tiled=True),
        lax.all_to_all(conv_out, "tp", split_axis=0, concat_axis=1, tiled=True),
    )
    weight_piece = lax.all_gather(stacked, "sp", axis=1, tiled=True)
    mixed = jnp.dot(
        rec_rows, weight_piece[:rec_width], preferred_element_type=jnp.float32
    ) + jnp.dot(conv_rows, weight_piece[rec_width:], preferred_element_type=jnp.float32)
    return mixed.astype(jnp.bfloat16)


def solution(mesh):
    return jax.shard_map(
        on_device,
        mesh=mesh,
        in_specs=(
            P("sp", None),
            P(),
            P("sp", "tp"),
            P("sp", "tp"),
            P("sp", "tp"),
            P("sp", "tp"),
            P("sp", "tp"),
            P("sp", "tp"),
            P("sp", "tp"),
            P(None, "tp"),
            P(None, "sp", "tp"),
            P(),
            P(None, "tp"),
            P("tp"),
            P("tp", "sp"),
            P("tp", "sp"),
        ),
        out_specs=P(("sp", "tp"), None),
        check_vma=False,
    )
```

profile of v0, /device:TPU:2, one launch (start us, length us, event | category | flops | bytes accessed | tf_op | source)
XLA Modules:
  0.0 441.9 jit_solution(4413109530318785613)
XLA Ops:
  11.3 7.4 %all_gather.61 = bf16[1024,256]{1,0:T(8,128)(2,1)S(1)} all-gather(bf16[256,256]{1,0:T(8,128)(2,1)} %param.38), channel_id=1, replica_groups=mesh['sp'=8,'tp'=4] {'tp'}, dimensions={0}, use_global_device_ids=true | all-gather | bytes 655360 | tf_op jit(solution)/shard_map/all_gather | solution.py:258
  18.7 7.3 %all_gather.62 = bf16[1024,256]{1,0:T(8,128)(2,1)S(1)} all-gather(bf16[256,256]{1,0:T(8,128)(2,1)S(1)} %copy-done.8), channel_id=1, replica_groups=mesh['sp'=8,'tp'=4] {'tp'}, dimensions={0}, use_global_device_ids=true | all-gather | bytes 655360 | tf_op jit(solution)/shard_map/all_gather | solution.py:259
  28.8 21.3 %all-gather.11.cloned.1.call-done = bf16[2048,256]{1,0:T(8,128)(2,1)} async-done(((bf16[256,256]{1,0:T(8,128)(2,1)}), bf16[2048,256]{1,0:T(8,128)(2,1)}) %all-gather.11.cloned.1.call-update) | async-done | bytes 1048592 | tf_op jit(solution)/shard_map/all_gather | solution.py:216
  54.3 37.0 %all-gather.17.cloned.1.call-done = bf16[2048,256]{1,0:T(8,128)(2,1)} async-done(((bf16[256,256]{1,0:T(8,128)(2,1)}), bf16[2048,256]{1,0:T(8,128)(2,1)}) %all-gather.17.cloned.1.call-update) | async-done | bytes 1048592 | tf_op jit(solution)/shard_map/all_gather | solution.py:217
  94.4 4.1 rev.16
  101.6 30.8 %all-gather.13.cloned.1.call-done = bf16[2048,256]{1,0:T(8,128)(2,1)} async-done(((bf16[256,256]{1,0:T(8,128)(2,1)}), bf16[2048,256]{1,0:T(8,128)(2,1)}) %all-gather.13.cloned.1.call-update) | async-done | bytes 1048592 | tf_op jit(solution)/shard_map/all_gather | solution.py:218
  138.2 33.3 %all-gather = bf16[16,128,128]{2,1,0:T(8,128)(2,1)} all-gather(bf16[2,128,128]{2,1,0:T(8,128)(2,1)S(1)} %convolution_convert_fusion.1), channel_id=2, replica_groups=mesh['sp'=8,'tp'=4] {'sp'}, dimensions={0}, use_global_device_ids=true | all-gather | bytes 589824 | tf_op jit(solution)/shard_map/all_gather | solution.py:21
  171.5 18.8 %all_gather.51 = bf16[8,2,128]{2,1,0:T(2,128)(2,1)S(1)} all-gather(bf16[1,2,128]{2,1,0:T(2,128)(2,1)S(1)} %copy.249), channel_id=1, replica_groups=mesh['sp'=8,'tp'=4] {'sp'}, dimensions={0}, use_global_device_ids=true | all-gather | bytes 4608 | tf_op jit(solution)/shard_map/all_gather | solution.py:21
  192.3 2.8 divide_multiply_fusion
  200.9 2.6 rev.18
  205.4 37.2 %all-gather.1 = bf16[16,128,128]{2,1,0:T(8,128)(2,1)} all-gather(bf16[2,128,128]{2,1,0:T(8,128)(2,1)S(1)} %convolution_convert_fusion), channel_id=3, replica_groups=mesh['sp'=8,'tp'=4] {'sp'}, dimensions={0}, use_global_device_ids=true | all-gather | bytes 589824 | tf_op jit(solution)/shard_map/all_gather | solution.py:21
  242.6 16.5 %all_gather.57 = bf16[8,2,128]{2,1,0:T(2,128)(2,1)S(1)} all-gather(bf16[1,2,128]{2,1,0:T(2,128)(2,1)S(1)} %slice.96), channel_id=1, replica_groups=mesh['sp'=8,'tp'=4] {'sp'}, dimensions={0}, use_global_device_ids=true | all-gather | bytes 4608 | tf_op jit(solution)/shard_map/all_gather | solution.py:21
  259.1 6.3 %while.53 = (s32[]{:T(128)}, f32[2,128,128]{2,1,0:T(8,128)S(1)}, s32[]{:T(128)}, bf16[8,2,128]{2,1,0:T(2,128)(2,1)S(1)}, bf16[8,2,128,128]{3,2,1,0:T(8,128)(2,1)...) while((s32[]{:T(128)}, f32[2,128,128]{2,1,0:T(8,128)S(1)}, s32[]{:T(128)}, ...), condition=%wide.region_11.12_spmd, body=%wide.region_10.11_spmd.sunk | while | flops 98566 | bytes 330387 | solution.py:38
  265.3 2.3 rev.19
  269.6 13.4 %while.55 = (s32[]{:T(128)}, f32[2,128,128]{2,1,0:T(8,128)S(1)}, f32[6,64,2,128]{3,1,0,2:T(8,128)S(1)}, f32[6,64,2,128]{3,2,1,0:T(2,128)S(1)}, f32[6,64,2,128]{3...) while((s32[]{:T(128)}, f32[2,128,128]{2,1,0:T(8,128)S(1)}, ...), condition=%wide.region_14.15_spmd.clone, body=%wide.region_12.14_spmd.clone.sunk | while | flops 76709888 | bytes 1644649 | solution.py:101
  283.3 18.4 %while.54 = (s32[]{:T(128)}, f32[2,128,128]{2,1,0:T(8,128)S(1)}, f32[6,64,2,128]{3,1,0,2:T(8,128)S(1)}, f32[6,64,2,128]{3,2,1,0:T(2,128)S(1)}, f32[6,64,2,128]{3...) while((s32[]{:T(128)}, f32[2,128,128]{2,1,0:T(8,128)S(1)}, ...), condition=%wide.region_7.8_spmd.clone, body=%wide.region_5.7_spmd.clone.sunk | while | flops 76709888 | bytes 1742949 | solution.py:101
  306.4 3.6 collective-permute-start
  310.0 5.3 %collective-permute-start.1 = (bf16[15,256]{0,1:T(8,128)(2,1)S(1)}, bf16[15,256]{0,1:T(8,128)(2,1)S(1)}, u32[]{:S(2)}, u32[]{:S(2)}) collective-permute-start(bf16[15,256]{0,1:T(8,128)(2,1)S(1)} %get-tuple-element.399), channel_id=1, source_target_pairs={{4,0},{8,4},{12,8},{16,12},{20,16},{24,20},{28,24},{5,1},{9,5},{13... | collective-permute-start | bytes 23048 | tf_op jit(solution)/shard_map/ppermute | solution.py:49
  318.2 3.5 all-to-all-start
  327.4 3.4 all-to-all-start.1
  330.8 5.2 %all-to-all-done.1 = bf16[4,96,256]{2,1,0:T(8,128)(2,1)S(1)} async-done(((bf16[4,96,256]{2,1,0:T(8,128)(2,1)}), bf16[4,96,256]{2,1,0:T(8,128)(2,1)S(1)}, u32[]{:S(2)}, u32[]{:S(2)}) %all-to-all-start.1) | async-done | bytes 196640 | tf_op jit(solution)/shard_map/all_to_all | solution.py:265
  336.1 92.3 %all-gather.21.cloned.1.call-done = bf16[2048,2048]{1,0:T(8,128)(2,1)} async-done(((bf16[2048,256]{1,0:T(8,128)(2,1)}), bf16[2048,2048]{1,0:T(8,128)(2,1)}) %all-gather.21.cloned.1.call-update) | async-done | bytes 8388624 | tf_op jit(solution)/shard_map/all_gather | solution.py:267
  428.4 3.0 fusion.36
  431.4 3.7 fusion.46
  (260 shorter events, 86.5 us)
Async XLA Ops:
  6.5 315.6 %copy-start = (bf16[31,256]{1,0:T(8,128)(2,1)S(1)}, bf16[31,256]{1,0:T(8,128)(2,1)}, u32[]{:S(2)}) copy-start(bf16[31,256]{1,0:T(8,128)(2,1)} %param.36) | copy-start | bytes 47620
  6.5 12.2 %copy-start.8 = (bf16[256,256]{1,0:T(8,128)(2,1)S(1)}, bf16[256,256]{1,0:T(8,128)(2,1)}, u32[]{:S(2)}) copy-start(bf16[256,256]{1,0:T(8,128)(2,1)} %param.39) | copy-start | bytes 393220
  6.5 43.6 %all-gather.11.cloned.1.call-start = ((), (), s32[]{:S(2)}) async-start(), calls=%async_computation.2 | async-start | bytes 1179648 | tf_op jit(solution)/shard_map/all_gather | solution.py:216
  7.3 84.0 %all-gather.17.cloned.1.call-start = ((), (), s32[]{:S(2)}) async-start(), calls=%async_computation.5 | async-start | bytes 1179648 | tf_op jit(solution)/shard_map/all_gather | solution.py:217
  8.0 124.4 %all-gather.13.cloned.1.call-start = ((), (), s32[]{:S(2)}) async-start(), calls=%async_computation.3 | async-start | bytes 1179648 | tf_op jit(solution)/shard_map/all_gather | solution.py:218
  8.7 183.5 %all-gather.15.cloned.1.call-start = ((), (), s32[]{:S(2)}) async-start(), calls=%async_computation.4 | async-start | bytes 1179648 | tf_op jit(solution)/shard_map/all_gather | solution.py:215
  9.3 292.9 %all-gather.25.cloned.1.call-start = ((), (), s32[]{:S(2)}) async-start(), calls=%async_computation.9 | async-start | bytes 1179648 | tf_op jit(solution)/shard_map/all_gather | solution.py:221
  9.9 294.4 %all-gather.23.cloned.1.call-start = ((), (), s32[]{:S(2)}) async-start(), calls=%async_computation.8 | async-start | bytes 1179648 | tf_op jit(solution)/shard_map/all_gather | solution.py:220
  10.5 304.8 %all-gather.19.cloned.1.call-start = ((), (), s32[]{:S(2)}) async-start(), calls=%async_computation.6 | async-start | bytes 1179648 | tf_op jit(solution)/shard_map/all_gather | solution.py:219
  11.2 417.1 %all-gather.21.cloned.1.call-start = ((), (), s32[]{:S(2)}) async-start(), calls=%async_computation.7 | async-start | bytes 9437184 | tf_op jit(solution)/shard_map/all_gather | solution.py:267
  26.0 1.2 copy-start.10
  26.0 1.8 copy-start.1
  27.1 1.1 copy-start.11
  27.1 1.1 copy-start.9
  27.1 1.3 copy-start.12
  27.1 1.3 copy-start.13
  138.2 53.1 %copy-start.7 = (f32[384,256]{1,0:T(8,128)S(1)}, f32[384,256]{1,0:T(8,128)}, u32[]{:S(2)}) copy-start(f32[384,256]{1,0:T(8,128)} %copy.253) | copy-start | bytes 1179652
  195.0 4.8 %copy-start.5 = (f32[6,64,2,128]{3,2,1,0:T(2,128)S(1)}, f32[6,64,2,128]{3,2,1,0:T(2,128)}, u32[]{:S(2)}) copy-start(f32[6,64,2,128]{3,2,1,0:T(2,128)} %copy-done.4) | copy-start | bytes 1179652
  203.6 61.8 %copy-start.6 = (f32[384,256]{0,1:T(8,128)S(1)}, f32[384,256]{0,1:T(8,128)}, u32[]{:S(2)}) copy-start(f32[384,256]{0,1:T(8,128)} %divide_multiply_fusion) | copy-start | bytes 1179652
  306.4 15.3 %collective-permute-start = (bf16[15,256]{0,1:T(8,128)(2,1)S(1)}, bf16[15,256]{0,1:T(8,128)(2,1)S(1)}, u32[]{:S(2)}, u32[]{:S(2)}) collective-permute-start(bf16[15,256]{0,1:T(8,128)(2,1)S(1)} %get-tuple-element.398), channel_id=1, source_target_pairs={{0,4},{4,8},{8,12},{12,16},{16,20},{20,24},{24,28},{1,5},{5,9},{9,... | collective-permute-start | bytes 23048 | tf_op jit(solution)/shard_map/ppermute | solution.py:46
  310.0 11.7 %collective-permute-start.1 = (bf16[15,256]{0,1:T(8,128)(2,1)S(1)}, bf16[15,256]{0,1:T(8,128)(2,1)S(1)}, u32[]{:S(2)}, u32[]{:S(2)}) collective-permute-start(bf16[15,256]{0,1:T(8,128)(2,1)S(1)} %get-tuple-element.399), channel_id=1, source_target_pairs={{4,0},{8,4},{12,8},{16,12},{20,16},{24,20},{28,24},{5,1},{9,5},{13... | collective-permute-start | bytes 23048 | tf_op jit(solution)/shard_map/ppermute | solution.py:49
  318.2 4.0 copy-start.14
  318.2 9.3 %all-to-all-start = ((bf16[4,96,256]{2,1,0:T(8,128)(2,1)}), bf16[4,96,256]{2,1,0:T(8,128)(2,1)S(1)}, u32[]{:S(2)}, u32[]{:S(2)}) async-start(bf16[4,96,256]{2,1,0:T(8,128)(2,1)} %bitcast.27), calls=%async_computation | async-start | bytes 393216 | tf_op jit(solution)/shard_map/all_to_all | solution.py:264
  327.4 8.6 %all-to-all-start.1 = ((bf16[4,96,256]{2,1,0:T(8,128)(2,1)}), bf16[4,96,256]{2,1,0:T(8,128)(2,1)S(1)}, u32[]{:S(2)}, u32[]{:S(2)}) async-start(bf16[4,96,256]{2,1,0:T(8,128)(2,1)} %multiply_convert_fusion), calls=%async_computation.1 | async-start | bytes 393216 | tf_op jit(solution)/shard_map/all_to_all | solution.py:265
  (3 other events, 2.5 us)
Sparse Core Ops, SparseCore 0:
  9.5 40.6 all-gather.10
  52.2 38.9 all-gather.16
  93.4 39.0 all-gather.12
  134.4 41.0 all-gather.14
  177.5 40.3 all-gather.24
  219.9 39.1 all-gather.22
  261.3 39.0 all-gather.18
  302.4 125.8 all-gather.20
where the time goes:
time: 446 us; the launch traced here: 442 us
  waiting for transfers between devices  191 us (43%)
  blocking collectives  120 us (27%)
  matrix products  39.3 us (9%)
  local copies, waits for them, and re-layouts  32.4 us (7%)
  other arithmetic  27.5 us (6%)
  starting transfers between devices  16 us (4%)
  between operations  14.1 us (3%)
    all_gather x4, blocking collectives, prefix(): lax.all_gather(a.astype(kind), axis)  106 us
    all_gather x1, waiting for transfers between devices, on_device(): weight_piece = lax.all_gather(stacked, 'sp', axis=1, tiled=True)  92.3 us
    all_gather x1, waiting for transfers between devices, on_device(): lax.all_gather(weights[2], 'sp', axis=0, tiled=True)  37 us
    all_gather x1, waiting for transfers between devices, on_device(): lax.all_gather(weights[3], 'sp', axis=0, tiled=True)  30.8 us
    all_gather x1, waiting for transfers between devices, on_device(): lax.all_gather(weights[1], 'sp', axis=0, tiled=True)  21.3 us
    dot_general x7, matrix products, on_device(): jnp.dot(normed, weight_piece, preferred_element_type=jnp.float32)  14.8 us
    rev x6, local copies, waits for them, and re-layouts, mix_direction(): jnp.flip(tensor, 0)  13 us
    mul x12, other arithmetic, advance(): lowered = gap_block * jnp.exp(-running_state)  11.9 us
  transfers between devices with their start and end apart: 12, of which 5 were waited for; matrix products, arithmetic and copies ran while one was open for 20% of the time, Pallas kernels for 0%

commit v1 on v0

v1 whole, which is shorter than its diff:
```python
import functools

import jax
import jax.numpy as jnp
from jax import lax
from jax.experimental import pallas as pl
from jax.experimental.pallas import tpu as pltpu
from jax.sharding import PartitionSpec as P

HEAD = 128
BLK = 128
MESH = pl.DeviceIdType.MESH
F32 = jnp.float32
BF16 = jnp.bfloat16
EDGE = 16


def dot(a, b, dims=((1,), (0,)), precision=None):
    return lax.dot_general(
        a, b, (dims, ((), ())), preferred_element_type=F32, precision=precision
    )


def kernel(
    ns, nt, nx, taps_n,
    x_ref, gain_ref, w_ref, slack_ref, extra_ref, sub_ref, taps_ref, cscale_ref, wo_ref,
    out_ref,
    win, wout, xs, acc, edge_out, edge_in, frame, lifted, local, decay, pack, st, osum, rec, conv,
    part, rbuf,
    in_send, in_recv, out_send, out_recv, halo_send, halo_recv, st_send, st_recv, rs_send, rs_recv,
):
    nz = ns // nx
    s = lax.axis_index("sp")
    t = lax.axis_index("tp")
    z = s // nx
    x = s % nx
    tl, d_model = x_ref.shape
    n_in, kc, ch = w_ref.shape
    nh = ch // HEAD
    nb = tl // BLK
    rows = tl // nt
    nc = wo_ref.shape[2]
    right = z * nx + lax.rem(x + 1, nx)

    barrier = pltpu.get_barrier_semaphore()

    @pl.loop(1, ns)
    def _(k):
        pl.semaphore_signal(
            barrier, inc=1, device_id=(lax.rem(s + k, ns), t), device_id_type=MESH
        )

    @pl.loop(1, nt)
    def _(k):
        pl.semaphore_signal(
            barrier, inc=1, device_id=(s, lax.rem(t + k, nt)), device_id_type=MESH
        )

    pl.semaphore_wait(barrier, ns - 1 + nt - 1)

    def remote(src, buf, b, sends, recvs, direction, to):
        return pltpu.make_async_remote_copy(
            src_ref=src, dst_ref=buf.at[b], send_sem=sends.at[direction, b],
            recv_sem=recvs.at[b], device_id=(to, t), device_id_type=MESH,
        )

    streams = ((w_ref, win, in_send, in_recv), (wo_ref, wout, out_send, out_recv))

    def up(i, b, src):
        own, buf, sends, recvs = streams[i]

        @pl.when(z + 1 < nz)
        def _():
            remote(src, buf, b, sends, recvs, 0, jnp.minimum(s + nx, ns - 1)).start()

    def down(i, b, src):
        own, buf, sends, recvs = streams[i]

        @pl.when(z > 0)
        def _():
            remote(src, buf, b, sends, recvs, 1, jnp.maximum(s - nx, 0)).start()

    def across(i, b, src):
        own, buf, sends, recvs = streams[i]
        if nx > 1:
            remote(src, buf, b, sends, recvs, 2, right).start()

    def arrive(i, b):
        own, buf, sends, recvs = streams[i]
        remote(buf.at[b], buf, b, sends, recvs, 0, right).wait_recv()

    def send_own(i):
        own = streams[i][0]
        up(i, s, own)
        down(i, s, own)
        across(i, s, own)

    def z_stage(i, d, use):
        buf = streams[i][1]

        @pl.when(z - d >= 0)
        def _():
            b = s - d * nx
            arrive(i, b)
            up(i, b, buf.at[b])
            across(i, b, buf.at[b])

        @pl.when(z + d < nz)
        def _():
            b = s + d * nx
            arrive(i, b)
            down(i, b, buf.at[b])
            across(i, b, buf.at[b])

        if use is not None:

            @pl.when(z - d >= 0)
            def _():
                use(s - d * nx)

            @pl.when(z + d < nz)
            def _():
                use(s + d * nx)

    def x_stage(i, d, use):
        buf = streams[i][1]
        for e in range(1, nx):
            column = lax.rem(x + nx - e, nx)

            def one(zz):
                b = zz * nx + column
                arrive(i, b)
                if e < nx - 1:
                    across(i, b, buf.at[b])
                if use is not None:
                    use(b)

            @pl.when(z - d >= 0)
            def _():
                one(z - d)

            if d > 0:

                @pl.when(z + d < nz)
                def _():
                    one(z + d)

    def finish(i):
        own, buf, sends, recvs = streams[i]
        for zz in range(nz):
            b = zz * nx + x

            @pl.when((z + 1 < nz) & (zz <= z))
            def _():
                remote(own, buf, b, sends, recvs, 0, right).wait_send()

            @pl.when((z > 0) & (zz >= z))
            def _():
                remote(own, buf, b, sends, recvs, 1, right).wait_send()

            for e in range(nx - 1):
                c = zz * nx + lax.rem(x + nx - e, nx)
                remote(own, buf, c, sends, recvs, 2, right).wait_send()

    send_own(0)

    floats = x_ref[...].astype(F32)
    factor = lax.rsqrt(jnp.mean(floats * floats, axis=-1, keepdims=True) + 1e-06)
    for b in range(ns):
        cols = slice(b * kc, (b + 1) * kc)
        xs[b] = (
            x_ref[:, cols].astype(F32) * factor * gain_ref[:, cols].astype(F32)
        ).astype(BF16)

    @pl.loop(0, n_in)
    def _(m):
        acc[m] = dot(xs[s], w_ref[m])

    def consume(b):
        @pl.loop(0, n_in)
        def _(m):
            acc[m] += dot(xs[b], win[b, m])

    for d in range(nz + 1):
        if 1 <= d < nz:
            z_stage(0, d, consume)
        if d == nz - 1:
            send_own(1)
        if d >= 1:
            x_stage(0, d - 1, consume)

    glu = acc[5] * jax.nn.sigmoid(acc[6])
    glu = glu.astype(BF16)
    edge_out[0] = glu[:EDGE]
    edge_out[1] = glu[tl - EDGE:]
    frame[EDGE:EDGE + tl] = glu.astype(F32)

    row_i = lax.broadcasted_iota(jnp.int32, (BLK, BLK), 0)
    col_i = lax.broadcasted_iota(jnp.int32, (BLK, BLK), 1)
    first_half = lax.broadcasted_iota(jnp.int32, (16, HEAD), 0) < 8

    for d in range(2):
        keep = (row_i >= col_i) if d == 0 else (row_i <= col_i)
        tri = keep.astype(F32)
        for h in range(nh):
            lanes = slice(h * HEAD, (h + 1) * HEAD)
            state = jnp.zeros((HEAD, HEAD), F32)
            before = jnp.zeros((1, HEAD), F32)
            order = range(nb) if d == 0 else range(nb - 1, -1, -1)
            for n in order:
                rs = slice(n * BLK, (n + 1) * BLK)
                gap = slack_ref[d:d + 1, lanes] * jax.nn.sigmoid(-acc[1 + d, rs, lanes])
                log_decay = jnp.log1p(-gap) + extra_ref[d, rs, h:h + 1]
                cum = dot(tri, log_decay, precision=lax.Precision.HIGHEST)
                mid = cum[BLK // 2:BLK // 2 + 1]
                total = cum[BLK - 1:] if d == 0 else cum[:1]
                centred = cum - mid
                q = acc[0, rs, lanes]
                q = q * jax.nn.sigmoid(q)
                raised = (q * jnp.exp(centred)).astype(BF16)
                lowered = (gap * jnp.exp(-centred)).astype(BF16)
                v = acc[3, rs, lanes].astype(BF16)
                scores = jnp.where(keep, dot(raised, lowered, ((1,), (1,))), 0.0)
                inside = dot(scores.astype(BF16), v)
                if d == 0:
                    osum[rs, lanes] = inside
                else:
                    osum[rs, lanes] += inside
                lifted[d, h, rs] = raised
                local[d, h, n] = state * jnp.exp(mid)
                decay[d, h, n] = jnp.broadcast_to(before + mid, (8, HEAD))
                added = dot(v, lowered, ((0,), (0,)))
                state = state * jnp.exp(total) + added * jnp.exp(total - mid)
                before = before + total
            pack[d, h, :HEAD] = state.astype(BF16)
            high = before.astype(BF16).astype(F32)
            pack[d, h, HEAD:] = jnp.where(first_half, high, before - high).astype(BF16)

    def state_copy(d, peer, slot):
        return pltpu.make_async_remote_copy(
            src_ref=pack.at[d], dst_ref=st.at[slot], send_sem=st_send.at[peer],
            recv_sem=st_recv.at[slot], device_id=(peer, t), device_id_type=MESH,
        )

    def halo_copy(side, peer):
        return pltpu.make_async_remote_copy(
            src_ref=edge_out.at[side], dst_ref=edge_in.at[1 - side], send_sem=halo_send.at[side],
            recv_sem=halo_recv.at[1 - side], device_id=(peer, t), device_id_type=MESH,
        )

    @pl.when(s > 0)
    def _():
        halo_copy(0, jnp.maximum(s - 1, 0)).start()

    @pl.when(s < ns - 1)
    def _():
        halo_copy(1, jnp.minimum(s + 1, ns - 1)).start()

    @pl.loop(s + 1, ns)
    def _(p):
        state_copy(0, p, s).start()

    @pl.loop(0, s)
    def _(p):
        state_copy(1, p, s).start()

    for d in range(1, nz):
        z_stage(1, d, None)

    @pl.when(s > 0)
    def _():
        halo_copy(1, 0).wait_recv()
        frame[:EDGE] = edge_in[0].astype(F32)

    @pl.when(s == 0)
    def _():
        frame[:EDGE] = jnp.zeros((EDGE, ch), F32)

    @pl.when(s < ns - 1)
    def _():
        halo_copy(0, 0).wait_recv()
        frame[EDGE + tl:] = edge_in[1].astype(F32)

    @pl.when(s == ns - 1)
    def _():
        frame[EDGE + tl:] = jnp.zeros((EDGE, ch), F32)

    off = EDGE - taps_n // 2
    step = 64
    for g in range(nh):
        lanes = slice(g * HEAD, (g + 1) * HEAD)
        taps = taps_ref[:, lanes].astype(F32)
        for r in range(0, tl, step):
            total = jnp.zeros((step, HEAD), F32)
            for j in range(taps_n):
                total += taps[j:j + 1] * frame[r + j + off:r + j + off + step, lanes]
            total = total - jnp.mean(total, axis=-1, keepdims=True)
            var = jnp.mean(total * total, axis=-1, keepdims=True)
            y = total * lax.rsqrt(var + 1e-05) * cscale_ref[:, lanes].astype(F32)
            conv[r:r + step, lanes] = (y * jax.nn.sigmoid(y)).astype(BF16)

    for d in range(nz):
        x_stage(1, d, None)

    def join(d, b, state):
        got = st[b].astype(F32)
        shrink = jnp.exp(got[:, HEAD:HEAD + 1] + got[:, HEAD + 8:HEAD + 9])
        return state * shrink + got[:, :HEAD]

    def ahead(b, state):
        state_copy(0, b, b).wait_recv()
        return join(0, b, state)

    def behind(k, state):
        b = ns - 1 - k
        state_copy(1, b, b).wait_recv()
        return join(1, b, state)

    zero = jnp.zeros((nh, HEAD, HEAD), F32)
    incoming = (lax.fori_loop(0, s, ahead, zero), lax.fori_loop(0, ns - 1 - s, behind, zero))

    for h in range(nh):
        lanes = slice(h * HEAD, (h + 1) * HEAD)
        for n in range(nb):
            rs = slice(n * BLK, (n + 1) * BLK)
            o = osum[rs, lanes]
            for d in range(2):
                full = local[d, h, n] + incoming[d][h] * jnp.exp(decay[d, h, n, :1])
                o += dot(lifted[d, h, rs], full.astype(BF16), ((1,), (1,)))
            norm = lax.rsqrt(jnp.mean(o * o, axis=-1, keepdims=True) + 1e-06)
            e = acc[4, rs, lanes]
            rec[rs, lanes] = (
                o * norm * sub_ref[...].astype(F32) * (e * jax.nn.sigmoid(e))
            ).astype(BF16)

    wout[s] = wo_ref[...]
    for b in range(ns):
        cols = slice(b * nc, (b + 1) * nc)
        y = dot(rec[...], wout[b, 0]) + dot(conv[...], wout[b, 1])
        y = y.astype(BF16)
        for k in range(nt):
            part[k, :, cols] = y[k * rows:(k + 1) * rows]

    def sum_copy(peer, slot):
        return pltpu.make_async_remote_copy(
            src_ref=part.at[peer], dst_ref=rbuf.at[slot], send_sem=rs_send.at[peer],
            recv_sem=rs_recv.at[slot], device_id=(s, peer), device_id_type=MESH,
        )

    for k in range(1, nt):
        sum_copy(lax.rem(t + k, nt), t).start()

    finish(0)
    finish(1)

    @pl.when(s > 0)
    def _():
        halo_copy(0, 0).wait_send()

    @pl.when(s < ns - 1)
    def _():
        halo_copy(1, 0).wait_send()

    @pl.loop(s + 1, ns)
    def _(p):
        state_copy(0, p, s).wait_send()

    @pl.loop(0, s)
    def _(p):
        state_copy(1, p, s).wait_send()

    for k in range(1, nt):
        peer = lax.rem(t + k, nt)
        sum_copy(peer, peer).wait_recv()

    total = part[t].astype(F32)
    for k in range(1, nt):
        total += rbuf[lax.rem(t + k, nt)].astype(F32)
    out_ref[...] = total.astype(BF16)
    for k in range(1, nt):
        peer = lax.rem(t + k, nt)
        sum_copy(peer, peer).wait_send()


def on_device(ns, nt, nx, x, gain, w0, w1, w2, w3, w4, w5, w6, slack, extra, sub, taps, cscale, wa, wb):
    weights = jnp.stack((w0, w1, w2, w3, w4, w5, w6))
    readout = jnp.stack((wa, wb))
    tl, d_model = x.shape
    n_in, kc, ch = weights.shape
    nh = ch // HEAD
    nb = tl // BLK
    nc = readout.shape[2]
    rows = tl // nt
    dma = pltpu.SemaphoreType.DMA
    vmem = pl.BlockSpec(memory_space=pltpu.VMEM)
    return pl.pallas_call(
        functools.partial(kernel, ns, nt, nx, taps.shape[0]),
        out_shape=jax.ShapeDtypeStruct((rows, d_model), BF16),
        in_specs=[vmem] * 9,
        out_specs=vmem,
        scratch_shapes=[
            pltpu.VMEM((ns, n_in, kc, ch), BF16),
            pltpu.VMEM((ns, 2, ch, nc), BF16),
            pltpu.VMEM((ns, tl, kc), BF16),
            pltpu.VMEM((n_in, tl, ch), F32),
            pltpu.VMEM((2, EDGE, ch), BF16),
            pltpu.VMEM((2, EDGE, ch), BF16),
            pltpu.VMEM((tl + 2 * EDGE, ch), F32),
            pltpu.VMEM((2, nh, tl, HEAD), BF16),
            pltpu.VMEM((2, nh, nb, HEAD, HEAD), F32),
            pltpu.VMEM((2, nh, nb, 8, HEAD), F32),
            pltpu.VMEM((2, nh, HEAD + 16, HEAD), BF16),
            pltpu.VMEM((ns, nh, HEAD + 16, HEAD), BF16),
            pltpu.VMEM((tl, ch), F32),
            pltpu.VMEM((tl, ch), BF16),
            pltpu.VMEM((tl, ch), BF16),
            pltpu.VMEM((nt, rows, d_model), BF16),
            pltpu.VMEM((nt, rows, d_model), BF16),
            dma((3, ns)), dma((ns,)), dma((3, ns)), dma((ns,)),
            dma((2,)), dma((2,)), dma((ns,)), dma((ns,)), dma((nt,)), dma((nt,)),
        ],
        compiler_params=pltpu.CompilerParams(
            collective_id=0, has_side_effects=True, vmem_limit_bytes=60 * 1024 * 1024
        ),
    )(
        x, gain.reshape(1, -1), weights, slack, extra, sub.reshape(1, -1), taps,
        cscale.reshape(1, -1), readout,
    )


def solution(mesh):
    ns, nt = mesh.shape["sp"], mesh.shape["tp"]
    nx = max(nt // 2, 1)
    return jax.shard_map(
        functools.partial(on_device, ns, nt, nx),
        mesh=mesh,
        in_specs=(
            P("sp", None),
            P(),
            P("sp", "tp"),
            P("sp", "tp"),
            P("sp", "tp"),
            P("sp", "tp"),
            P("sp", "tp"),
            P("sp", "tp"),
            P("sp", "tp"),
            P(None, "tp"),
            P(None, "sp", "tp"),
            P(),
            P(None, "tp"),
            P("tp"),
            P("tp", "sp"),
            P("tp", "sp"),
        ),
        out_specs=P(("sp", "tp"), None),
        check_vma=False,
    )
```

time: 446 us -> 156 us (0.35)
  waiting for transfers between devices: 191 us -> 0 us
  Pallas kernels: 0 us -> 143 us
  blocking collectives: 120 us -> 0 us
  matrix products: 39.3 us -> 0 us
  other arithmetic: 27.5 us -> 0.72 us
  local copies, waits for them, and re-layouts: 32.4 us -> 9.58 us
  starting transfers between devices: 16 us -> 0 us
  between operations: 14.1 us -> 0.09 us
    all_gather x8 -> x0, waiting for transfers between devices: 181 us -> none  [the longest x1 92.3 us: on_device(): weight_piece = lax.all_gather(stacked, 'sp', axis=1, tiled=True)]
    pallas_call x0 -> x1, Pallas kernels: none -> 143 us  [on_device(): pl.pallas_call(functools.partial(kernel, ns, nt, nx, taps.shape[0]), out_...]
    all_gather x6 -> x0, blocking collectives: 120 us -> none  [the longest x4 106 us: prefix(): lax.all_gather(a.astype(kind), axis)]
    dot_general x59 -> x0, matrix products: 38.4 us -> none  [the longest x7 14.8 us: on_device(): jnp.dot(normed, weight_piece, preferred_element_type=jnp.float32)]
    rev x7 -> x0, local copies, waits for them, and re-layouts: 13.2 us -> none  [the longest x6 13 us: mix_direction(): jnp.flip(tensor, 0)]
    mul x14 -> x0, other arithmetic: 13.1 us -> none  [the longest x12 11.9 us: advance(): lowered = gap_block * jnp.exp(-running_state)]
    ppermute x2 -> x0, starting transfers between devices: 8.86 us -> none  [the longest x1 5.27 us: extended(): lax.ppermute(lax.slice_in_dim(block, 0, width, axis=dim), axis, backward)]
    add x11 -> x0, other arithmetic: 8.53 us -> none  [the longest x7 6.73 us: join_segments(): jnp.exp(later[0])[:, :, None] * earlier[1] + later[1]]
  transfers between devices with their start and end apart: 12 -> 0, of which waited for: 5 -> 0; matrix products, arithmetic and copies ran while one was open for 20% -> 0% of each run, Pallas kernels for 0% -> 0%
where the time goes in v1:
time: 156 us; the launch traced here: 153 us
  Pallas kernels  143 us (92%)
  local copies, waits for them, and re-layouts  9.58 us (6%)
    pallas_call x1, Pallas kernels, on_device(): pl.pallas_call(functools.partial(kernel, ns, nt, nx, taps.shape[0]), out_...  143 us
    unnamed x22, local copies, waits for them, and re-layouts  8.39 us

profile of v1, /device:TPU:2, one launch (start us, length us, event | category | flops | bytes accessed | tf_op | source)
XLA Modules:
  0.0 153.4 jit_solution(13275438932469097945)
XLA Ops:
  0.0 0.0 copy-start.1
  0.0 0.0 copy-start.2
  0.0 0.0 copy-start.5
  0.0 0.0 copy-start.6
  0.0 1.0 bitcast_dynamic-update-slice_fusion.6
  1.0 0.9 bitcast_dynamic-update-slice_fusion.5
  1.9 0.9 bitcast_dynamic-update-slice_fusion.4
  2.9 0.9 bitcast_dynamic-update-slice_fusion.3
  3.8 0.9 bitcast_dynamic-update-slice_fusion.2
  4.7 0.9 bitcast_dynamic-update-slice_fusion.1
  5.6 0.0 copy-done.1
  5.6 0.0 copy-done.4
  5.7 0.0 copy-start
  5.7 1.0 copy.17.extra_ref
  6.7 0.0 copy-done.3
  6.7 0.0 copy-done.2
  6.7 0.7 pad_maximum_fusion.wo_ref
  7.4 0.0 copy-done.5
  7.4 0.6 reshape.9.gain_ref
  8.0 0.0 copy-done.6
  8.0 0.6 reshape.11.cscale_ref
  8.6 0.0 copy-done
  8.6 143.0 %shard_map.154 = bf16[96,2048]{1,0:T(8,128)(2,1)} custom-call(bf16[384,2048]{1,0:T(8,128)(2,1)} %x_ref.1, bf16[1,2048]{1,0:T(2,128)(2,1)} %reshape.9.gain_ref, bf16[7,256,256]{2,1,0:T(8,128)(2,1)} %copy-done, f32[2,256]{1,0:T(2,128)} %slack_ref.1, f32[2,384,2]{2,1,0:T(8,128)} %copy.17.extra_ref, bf16[1,128]{1,0:T(2,128)(2,1)} %bitcast.19, ...), custom_call_target="tpu_custom_call" | custom-call | tf_op jit(solution)/shard_map/pallas_call | solution.py:396
  151.7 1.8 %copy.25 = bf16[96,2048]{1,0:T(8,128)(2,1)} copy(bf16[96,2048]{1,0:T(8,128)(2,1)} %shard_map.154) | data formatting | bytes 786432
  (3 shorter events, 0.0 us)
Async XLA Ops:
  0.0 5.6 %copy-start.1 = (bf16[256,256]{1,0:T(8,128)(2,1)S(1)}, bf16[256,256]{1,0:T(8,128)(2,1)}, u32[]{:S(2)}) copy-start(bf16[256,256]{1,0:T(8,128)(2,1)} %param.24) | copy-start | bytes 393220
  0.0 5.6 %copy-start.4 = (f32[2,384,2]{1,2,0:T(2,128)S(1)}, f32[2,384,2]{1,2,0:T(2,128)}, u32[]{:S(2)}) copy-start(f32[2,384,2]{1,2,0:T(2,128)} %param.26) | copy-start | bytes 18436
  0.0 6.7 %copy-start.3 = (bf16[256,256]{1,0:T(8,128)(2,1)S(1)}, bf16[256,256]{1,0:T(8,128)(2,1)}, u32[]{:S(2)}) copy-start(bf16[256,256]{1,0:T(8,128)(2,1)} %param.30) | copy-start | bytes 393220
  0.0 6.7 %copy-start.2 = (bf16[256,256]{1,0:T(8,128)(2,1)S(1)}, bf16[256,256]{1,0:T(8,128)(2,1)}, u32[]{:S(2)}) copy-start(bf16[256,256]{1,0:T(8,128)(2,1)} %param.31) | copy-start | bytes 393220
  0.0 7.4 %copy-start.5 = (bf16[2048]{0:T(1024)(128)(2,1)S(1)}, bf16[2048]{0:T(1024)(128)(2,1)}, u32[]{:S(2)}) copy-start(bf16[2048]{0:T(1024)(128)(2,1)} %param.17) | copy-start | bytes 12292
  0.0 8.0 %copy-start.6 = (bf16[256]{0:T(256)(128)(2,1)S(1)}, bf16[256]{0:T(256)(128)(2,1)}, u32[]{:S(2)}) copy-start(bf16[256]{0:T(256)(128)(2,1)} %param.29) | copy-start | bytes 1540
  5.7 3.0 %copy-start = (bf16[7,256,256]{2,1,0:T(8,128)(2,1)}, bf16[7,256,256]{2,1,0:T(8,128)(2,1)S(1)}, u32[]{:S(2)}) copy-start(bf16[7,256,256]{2,1,0:T(8,128)(2,1)S(1)} %bitcast_dynamic-update-slice_fusion.w_ref) | copy-start | bytes 2752516

commit v2 on v1

--- a/solution.py
+++ b/solution.py
@@ -23,11 +23,21 @@
 
 def kernel(
     ns, nt, nx, taps_n,
-    x_ref, gain_ref, w_ref, slack_ref, extra_ref, sub_ref, taps_ref, cscale_ref, wo_ref,
+    *refs,
+):
+    w_refs = refs[:9]
+    kernel_body(ns, nt, nx, taps_n, w_refs, *refs[9:])
+
+
+def kernel_body(
+    ns, nt, nx, taps_n, w_refs,
+    x_hbm, gain_ref, slack_ref, extra_ref, sub_ref, taps_ref, cscale_ref,
     out_ref,
-    win, wout, xs, acc, edge_out, edge_in, frame, lifted, local, decay, pack, st, osum, rec, conv,
-    part, rbuf,
-    in_send, in_recv, out_send, out_recv, halo_send, halo_recv, st_send, st_recv, rs_send, rs_recv,
+    x_ref,
+    win_a, win_b, wout, xs, acc, edge_out, edge_in, frame, lifted, local, decay, pack, st, osum, rec, conv,
+    part, cbuf, final, part2, rbuf,
+    a_send, a_recv, b_send, b_recv, out_send, out_recv, halo_send, halo_recv, st_send, st_recv, c_send, c_recv,
+    y_send, y_recv, load_sem,
 ):
     nz = ns // nx
     s = lax.axis_index("sp")
@@ -35,12 +45,22 @@
     z = s // nx
     x = s % nx
     tl, d_model = x_ref.shape
-    n_in, kc, ch = w_ref.shape
+    n_a, kc, ch = win_a.shape[1:]
+    n_b = win_b.shape[1]
     nh = ch // HEAD
     nb = tl // BLK
     rows = tl // nt
-    nc = wo_ref.shape[2]
+    nc = wout.shape[3]
     right = z * nx + lax.rem(x + 1, nx)
+
+    loads = [
+        pltpu.make_async_copy(w_refs[m], buf.at[s, m - base], load_sem.at[m])
+        for buf, base, count in ((win_a, 0, n_a), (win_b, n_a, n_b), (wout, n_a + n_b, 2))
+        for m in range(base, base + count)
+    ]
+    loads.append(pltpu.make_async_copy(x_hbm, x_ref, load_sem.at[n_a + n_b + 2]))
+    for load in loads:
+        load.start()
 
     barrier = pltpu.get_barrier_semaphore()
 
@@ -64,7 +84,11 @@
             recv_sem=recvs.at[b], device_id=(to, t), device_id_type=MESH,
         )
 
-    streams = ((w_ref, win, in_send, in_recv), (wo_ref, wout, out_send, out_recv))
+    streams = (
+        (win_a.at[s], win_a, a_send, a_recv),
+        (win_b.at[s], win_b, b_send, b_recv),
+        (wout.at[s], wout, out_send, out_recv),
+    )
 
     def up(i, b, src):
         own, buf, sends, recvs = streams[i]
@@ -121,6 +145,30 @@
             @pl.when(z + d < nz)
             def _():
                 use(s + d * nx)
+
+    def wide_first():
+        for e in range(1, nx):
+            b = z * nx + lax.rem(x + nx - e, nx)
+            arrive(2, b)
+            if e < nx - 1:
+                across(2, b, wout.at[b])
+            up(2, b, wout.at[b])
+            down(2, b, wout.at[b])
+
+    def wide_stage(d):
+        for column in range(nx):
+
+            @pl.when(z - d >= 0)
+            def _():
+                b = (z - d) * nx + column
+                arrive(2, b)
+                up(2, b, wout.at[b])
+
+            @pl.when(z + d < nz)
+            def _():
+                b = (z + d) * nx + column
+                arrive(2, b)
+                down(2, b, wout.at[b])
 
     def x_stage(i, d, use):
         buf = streams[i][1]
@@ -162,7 +210,29 @@
                 c = zz * nx + lax.rem(x + nx - e, nx)
                 remote(own, buf, c, sends, recvs, 2, right).wait_send()
 
+    def wide_finish():
+        own, buf, sends, recvs = streams[2]
+        for zz in range(nz):
+            for column in range(nx):
+                b = zz * nx + column
+
+                @pl.when((z + 1 < nz) & (zz <= z))
+                def _():
+                    remote(own, buf, b, sends, recvs, 0, right).wait_send()
+
+                @pl.when((z > 0) & (zz >= z))
+                def _():
+                    remote(own, buf, b, sends, recvs, 1, right).wait_send()
+
+        for e in range(nx - 1):
+            c = z * nx + lax.rem(x + nx - e, nx)
+            remote(own, buf, c, sends, recvs, 2, right).wait_send()
+
+    for load in loads[:n_a]:
+        load.wait()
     send_own(0)
+    for load in loads[n_a:]:
+        load.wait()
 
     floats = x_ref[...].astype(F32)
     factor = lax.rsqrt(jnp.mean(floats * floats, axis=-1, keepdims=True) + 1e-06)
@@ -172,33 +242,38 @@
             x_ref[:, cols].astype(F32) * factor * gain_ref[:, cols].astype(F32)
         ).astype(BF16)
 
-    @pl.loop(0, n_in)
+    @pl.loop(0, n_a)
     def _(m):
-        acc[m] = dot(xs[s], w_ref[m])
-
-    def consume(b):
-        @pl.loop(0, n_in)
+        acc[m] = dot(xs[s], win_a[s, m])
+
+    @pl.loop(0, n_b)
+    def _(m):
+        acc[n_a + m] = dot(xs[s], win_b[s, m])
+
+    def consume_a(b):
+        @pl.loop(0, n_a)
         def _(m):
-            acc[m] += dot(xs[b], win[b, m])
+            acc[m] += dot(xs[b], win_a[b, m])
+
+    def consume_b(b):
+        @pl.loop(0, n_b)
+        def _(m):
+            acc[n_a + m] += dot(xs[b], win_b[b, m])
 
     for d in range(nz + 1):
         if 1 <= d < nz:
-            z_stage(0, d, consume)
+            z_stage(0, d, consume_a)
         if d == nz - 1:
+            across(2, s, wout.at[s])
             send_own(1)
         if d >= 1:
-            x_stage(0, d - 1, consume)
-
-    glu = acc[5] * jax.nn.sigmoid(acc[6])
-    glu = glu.astype(BF16)
-    edge_out[0] = glu[:EDGE]
-    edge_out[1] = glu[tl - EDGE:]
-    frame[EDGE:EDGE + tl] = glu.astype(F32)
+            x_stage(0, d - 1, consume_a)
 
     row_i = lax.broadcasted_iota(jnp.int32, (BLK, BLK), 0)
     col_i = lax.broadcasted_iota(jnp.int32, (BLK, BLK), 1)
     first_half = lax.broadcasted_iota(jnp.int32, (16, HEAD), 0) < 8
 
+    z_done = 1
     for d in range(2):
         keep = (row_i >= col_i) if d == 0 else (row_i <= col_i)
         tri = keep.astype(F32)
@@ -235,6 +310,9 @@
             pack[d, h, :HEAD] = state.astype(BF16)
             high = before.astype(BF16).astype(F32)
             pack[d, h, HEAD:] = jnp.where(first_half, high, before - high).astype(BF16)
+            if (d * nh + h) % 2 == 0 and z_done < nz:
+                z_stage(1, z_done, consume_b)
+                z_done += 1
 
     def state_copy(d, peer, slot):
         return pltpu.make_async_remote_copy(
@@ -248,14 +326,6 @@
             recv_sem=halo_recv.at[1 - side], device_id=(peer, t), device_id_type=MESH,
         )
 
-    @pl.when(s > 0)
-    def _():
-        halo_copy(0, jnp.maximum(s - 1, 0)).start()
-
-    @pl.when(s < ns - 1)
-    def _():
-        halo_copy(1, jnp.minimum(s + 1, ns - 1)).start()
-
     @pl.loop(s + 1, ns)
     def _(p):
         state_copy(0, p, s).start()
@@ -264,8 +334,62 @@
     def _(p):
         state_copy(1, p, s).start()
 
-    for d in range(1, nz):
-        z_stage(1, d, None)
+    for d in range(z_done, nz):
+        z_stage(1, d, consume_b)
+    up(2, s, wout.at[s])
+    down(2, s, wout.at[s])
+    wide_first()
+    for d in range(min(2, nz)):
+        x_stage(1, d, consume_b)
+
+    def join(d, b, state):
+        got = st[b].astype(F32)
+        shrink = jnp.exp(got[:, HEAD:HEAD + 1] + got[:, HEAD + 8:HEAD + 9])
+        return state * shrink + got[:, :HEAD]
+
+    def ahead(b, state):
+        state_copy(0, b, b).wait_recv()
+        return join(0, b, state)
+
+    def behind(k, state):
+        b = ns - 1 - k
+        state_copy(1, b, b).wait_recv()
+        return join(1, b, state)
+
+    zero = jnp.zeros((nh, HEAD, HEAD), F32)
+    incoming = (lax.fori_loop(0, s, ahead, zero), lax.fori_loop(0, ns - 1 - s, behind, zero))
+
+    for h in range(nh):
+        lanes = slice(h * HEAD, (h + 1) * HEAD)
+        for n in range(nb):
+            rs = slice(n * BLK, (n + 1) * BLK)
+            o = osum[rs, lanes]
+            for d in range(2):
+                full = local[d, h, n] + incoming[d][h] * jnp.exp(decay[d, h, n, :1])
+                o += dot(lifted[d, h, rs], full.astype(BF16), ((1,), (1,)))
+            norm = lax.rsqrt(jnp.mean(o * o, axis=-1, keepdims=True) + 1e-06)
+            osum[rs, lanes] = o * norm * sub_ref[...].astype(F32)
+
+    for d in range(2, nz):
+        wide_stage(d - 1)
+        x_stage(1, d, consume_b)
+
+    glu = acc[n_a + 1] * jax.nn.sigmoid(acc[n_a + 2])
+    glu = glu.astype(BF16)
+    edge_out[0] = glu[:EDGE]
+    edge_out[1] = glu[tl - EDGE:]
+    frame[EDGE:EDGE + tl] = glu.astype(F32)
+
+    @pl.when(s > 0)
+    def _():
+        halo_copy(0, jnp.maximum(s - 1, 0)).start()
+
+    @pl.when(s < ns - 1)
+    def _():
+        halo_copy(1, jnp.minimum(s + 1, ns - 1)).start()
+
+    e = acc[n_a]
+    rec[...] = (osum[...] * (e * jax.nn.sigmoid(e))).astype(BF16)
 
     @pl.when(s > 0)
     def _():
@@ -299,59 +423,48 @@
             y = total * lax.rsqrt(var + 1e-05) * cscale_ref[:, lanes].astype(F32)
             conv[r:r + step, lanes] = (y * jax.nn.sigmoid(y)).astype(BF16)
 
-    for d in range(nz):
-        x_stage(1, d, None)
-
-    def join(d, b, state):
-        got = st[b].astype(F32)
-        shrink = jnp.exp(got[:, HEAD:HEAD + 1] + got[:, HEAD + 8:HEAD + 9])
-        return state * shrink + got[:, :HEAD]
-
-    def ahead(b, state):
-        state_copy(0, b, b).wait_recv()
-        return join(0, b, state)
-
-    def behind(k, state):
-        b = ns - 1 - k
-        state_copy(1, b, b).wait_recv()
-        return join(1, b, state)
-
-    zero = jnp.zeros((nh, HEAD, HEAD), F32)
-    incoming = (lax.fori_loop(0, s, ahead, zero), lax.fori_loop(0, ns - 1 - s, behind, zero))
-
-    for h in range(nh):
-        lanes = slice(h * HEAD, (h + 1) * HEAD)
-        for n in range(nb):
-            rs = slice(n * BLK, (n + 1) * BLK)
-            o = osum[rs, lanes]
-            for d in range(2):
-                full = local[d, h, n] + incoming[d][h] * jnp.exp(decay[d, h, n, :1])
-                o += dot(lifted[d, h, rs], full.astype(BF16), ((1,), (1,)))
-            norm = lax.rsqrt(jnp.mean(o * o, axis=-1, keepdims=True) + 1e-06)
-            e = acc[4, rs, lanes]
-            rec[rs, lanes] = (
-                o * norm * sub_ref[...].astype(F32) * (e * jax.nn.sigmoid(e))
-            ).astype(BF16)
-
-    wout[s] = wo_ref[...]
-    for b in range(ns):
-        cols = slice(b * nc, (b + 1) * nc)
+    if nz > 1:
+        wide_stage(nz - 1)
+
+    half = nt // 2
+    mine = lax.rem(t, 2)
+    place = t // 2
+    other = 1 - mine
+
+    def core_copy(b):
+        return pltpu.make_async_remote_copy(
+            src_ref=part.at[b, other], dst_ref=cbuf.at[b], send_sem=c_send.at[b],
+            recv_sem=c_recv.at[b], device_id=(s, 2 * place + other), device_id_type=MESH,
+        )
+
+    def y_copy(b, peer, slot):
+        return pltpu.make_async_remote_copy(
+            src_ref=part2.at[b, peer], dst_ref=rbuf.at[b, slot], send_sem=y_send.at[b, peer],
+            recv_sem=y_recv.at[b, slot], device_id=(s, 2 * peer + mine), device_id_type=MESH,
+        )
+
+    @pl.loop(0, ns)
+    def _(b):
         y = dot(rec[...], wout[b, 0]) + dot(conv[...], wout[b, 1])
         y = y.astype(BF16)
         for k in range(nt):
-            part[k, :, cols] = y[k * rows:(k + 1) * rows]
-
-    def sum_copy(peer, slot):
-        return pltpu.make_async_remote_copy(
-            src_ref=part.at[peer], dst_ref=rbuf.at[slot], send_sem=rs_send.at[peer],
-            recv_sem=rs_recv.at[slot], device_id=(s, peer), device_id_type=MESH,
-        )
-
-    for k in range(1, nt):
-        sum_copy(lax.rem(t + k, nt), t).start()
+            part[b, k % 2, k // 2] = y[k * rows:(k + 1) * rows]
+        core_copy(b).start()
+
+    @pl.loop(0, ns)
+    def _(b):
+        core_copy(b).wait_recv()
+        for k in range(1, half):
+            peer = lax.rem(place + k, half)
+            part2[b, peer] = (
+                part[b, mine, peer].astype(F32) + cbuf[b, peer].astype(F32)
+            ).astype(BF16)
+            y_copy(b, peer, place).start()
+        final[b] = part[b, mine, place].astype(F32) + cbuf[b, place].astype(F32)
 
     finish(0)
     finish(1)
+    wide_finish()
 
     @pl.when(s > 0)
     def _():
@@ -369,40 +482,45 @@
     def _(p):
         state_copy(1, p, s).wait_send()
 
-    for k in range(1, nt):
-        peer = lax.rem(t + k, nt)
-        sum_copy(peer, peer).wait_recv()
-
-    total = part[t].astype(F32)
-    for k in range(1, nt):
-        total += rbuf[lax.rem(t + k, nt)].astype(F32)
-    out_ref[...] = total.astype(BF16)
-    for k in range(1, nt):
-        peer = lax.rem(t + k, nt)
-        sum_copy(peer, peer).wait_send()
+    for b in range(ns):
+        total = final[b]
+        for k in range(1, half):
+            peer = lax.rem(place + k, half)
+            y_copy(b, peer, peer).wait_recv()
+            total += rbuf[b, peer].astype(F32)
+        out_ref[:, b * nc:(b + 1) * nc] = total.astype(BF16)
+
+    @pl.loop(0, ns)
+    def _(b):
+        core_copy(b).wait_send()
+        for k in range(1, half):
+            peer = lax.rem(place + k, half)
+            y_copy(b, peer, peer).wait_send()
 
 
 def on_device(ns, nt, nx, x, gain, w0, w1, w2, w3, w4, w5, w6, slack, extra, sub, taps, cscale, wa, wb):
-    weights = jnp.stack((w0, w1, w2, w3, w4, w5, w6))
-    readout = jnp.stack((wa, wb))
     tl, d_model = x.shape
-    n_in, kc, ch = weights.shape
+    n_a, n_b = 4, 3
+    kc, ch = w0.shape
     nh = ch // HEAD
     nb = tl // BLK
-    nc = readout.shape[2]
+    nc = wa.shape[1]
     rows = tl // nt
+    half = nt // 2
     dma = pltpu.SemaphoreType.DMA
     vmem = pl.BlockSpec(memory_space=pltpu.VMEM)
     return pl.pallas_call(
         functools.partial(kernel, ns, nt, nx, taps.shape[0]),
         out_shape=jax.ShapeDtypeStruct((rows, d_model), BF16),
-        in_specs=[vmem] * 9,
+        in_specs=[pl.BlockSpec(memory_space=pl.ANY)] * 10 + [vmem] * 6,
         out_specs=vmem,
         scratch_shapes=[
-            pltpu.VMEM((ns, n_in, kc, ch), BF16),
+            pltpu.VMEM((tl, d_model), BF16),
+            pltpu.VMEM((ns, n_a, kc, ch), BF16),
+            pltpu.VMEM((ns, n_b, kc, ch), BF16),
             pltpu.VMEM((ns, 2, ch, nc), BF16),
             pltpu.VMEM((ns, tl, kc), BF16),
-            pltpu.VMEM((n_in, tl, ch), F32),
+            pltpu.VMEM((n_a + n_b, tl, ch), F32),
             pltpu.VMEM((2, EDGE, ch), BF16),
             pltpu.VMEM((2, EDGE, ch), BF16),
             pltpu.VMEM((tl + 2 * EDGE, ch), F32),
@@ -414,17 +532,21 @@
             pltpu.VMEM((tl, ch), F32),
             pltpu.VMEM((tl, ch), BF16),
             pltpu.VMEM((tl, ch), BF16),
-            pltpu.VMEM((nt, rows, d_model), BF16),
-            pltpu.VMEM((nt, rows, d_model), BF16),
-            dma((3, ns)), dma((ns,)), dma((3, ns)), dma((ns,)),
-            dma((2,)), dma((2,)), dma((ns,)), dma((ns,)), dma((nt,)), dma((nt,)),
+            pltpu.VMEM((ns, 2, half, rows, nc), BF16),
+            pltpu.VMEM((ns, half, rows, nc), BF16),
+            pltpu.VMEM((ns, rows, nc), F32),
+            pltpu.VMEM((ns, half, rows, nc), BF16),
+            pltpu.VMEM((ns, half, rows, nc), BF16),
+            dma((3, ns)), dma((ns,)), dma((3, ns)), dma((ns,)), dma((3, ns)), dma((ns,)),
+            dma((2,)), dma((2,)), dma((ns,)), dma((ns,)), dma((ns,)), dma((ns,)),
+            dma((ns, half)), dma((ns, half)), dma((10,)),
         ],
         compiler_params=pltpu.CompilerParams(
             collective_id=0, has_side_effects=True, vmem_limit_bytes=60 * 1024 * 1024
         ),
     )(
-        x, gain.reshape(1, -1), weights, slack, extra, sub.reshape(1, -1), taps,
-        cscale.reshape(1, -1), readout,
+        w0, w1, w2, w3, w4, w5, w6, wa, wb, x, gain.reshape(1, -1), slack, extra,
+        sub.reshape(1, -1), taps, cscale.reshape(1, -1),
     )
 
 

time: 156 us -> 145 us (0.929); the launches traced: 153 us -> 145 us
  Pallas kernels: 143 us -> 139 us
  local copies, waits for them, and re-layouts: 9.58 us -> 5.87 us
    unnamed x22 -> x2, local copies, waits for them, and re-layouts: 8.39 us -> 3.39 us
    pallas_call x1, Pallas kernels: 143 us -> 139 us  [on_device(): pl.pallas_call(functools.partial(kernel, ns, nt, nx, taps.shape[0]), out_...]
where the time goes in v2:
time: 145 us
  Pallas kernels  139 us (96%)
  local copies, waits for them, and re-layouts  5.87 us (4%)
    pallas_call x1, Pallas kernels, on_device(): pl.pallas_call(functools.partial(kernel, ns, nt, nx, taps.shape[0]), out_...  139 us
    unnamed x2, local copies, waits for them, and re-layouts  3.39 us

profile of v2, /device:TPU:2, one launch (start us, length us, event | category | flops | bytes accessed | tf_op | source)
XLA Modules:
  0.0 144.6 jit_solution(13773645791174199260)
XLA Ops:
  0.0 1.2 reshape.11.refs_15_
  1.2 1.3 reshape.9.refs_10_
  2.5 1.6 %copy.17.refs_12_ = f32[2,384,2]{2,1,0:T(8,128)} copy(f32[2,384,2]{1,2,0:T(2,128)} %param.26) | data formatting | bytes 12288 | tf_op args[10]
  4.1 138.7 %shard_map.154 = bf16[96,2048]{1,0:T(8,128)(2,1)} custom-call(bf16[256,256]{1,0:T(8,128)(2,1)} %refs_0_.1, bf16[256,256]{1,0:T(8,128)(2,1)} %refs_1_.1, bf16[256,256]{1,0:T(8,128)(2,1)} %refs_2_.1, bf16[256,256]{1,0:T(8,128)(2,1)} %refs_3_.1, bf16[256,256]{1,0:T(8,128)(2,1)} %refs_4_.1, bf16[256,256]{1,0:T(8,128)(2,1)} %refs_5_.1, bf16[256,256]{1,0:T(8,128)(2,1)} %refs_6_.1, ...), custom_call_target="tpu_custom_call" | custom-call | tf_op jit(solution)/shard_map/pallas_call | solution.py:512
  142.8 1.8 %copy.19 = bf16[96,2048]{1,0:T(8,128)(2,1)} copy(bf16[96,2048]{1,0:T(8,128)(2,1)} %shard_map.154) | data formatting | bytes 786432

commit v3 on v2

--- a/solution.py
+++ b/solution.py
@@ -260,14 +260,12 @@
         def _(m):
             acc[n_a + m] += dot(xs[b], win_b[b, m])
 
-    for d in range(nz + 1):
-        if 1 <= d < nz:
-            z_stage(0, d, consume_a)
-        if d == nz - 1:
-            across(2, s, wout.at[s])
-            send_own(1)
-        if d >= 1:
-            x_stage(0, d - 1, consume_a)
+    for d in range(1, nz):
+        z_stage(0, d, consume_a)
+    across(2, s, wout.at[s])
+    send_own(1)
+    for d in range(nz):
+        x_stage(0, d, consume_a)
 
     row_i = lax.broadcasted_iota(jnp.int32, (BLK, BLK), 0)
     col_i = lax.broadcasted_iota(jnp.int32, (BLK, BLK), 1)
@@ -339,8 +337,11 @@
     up(2, s, wout.at[s])
     down(2, s, wout.at[s])
     wide_first()
-    for d in range(min(2, nz)):
-        x_stage(1, d, consume_b)
+    x_stage(1, 0, consume_b)
+    if nz > 1:
+        if nz > 2:
+            wide_stage(1)
+        x_stage(1, 1, consume_b)
 
     def join(d, b, state):
         got = st[b].astype(F32)
@@ -371,7 +372,8 @@
             osum[rs, lanes] = o * norm * sub_ref[...].astype(F32)
 
     for d in range(2, nz):
-        wide_stage(d - 1)
+        if d > 2:
+            wide_stage(d - 1)
         x_stage(1, d, consume_b)
 
     glu = acc[n_a + 1] * jax.nn.sigmoid(acc[n_a + 2])

time: 145 us -> 139 us (0.959)
  Pallas kernels: 139 us -> 132 us
    pallas_call x1, Pallas kernels: 139 us -> 132 us  [on_device(): pl.pallas_call(functools.partial(kernel, ns, nt, nx, taps.shape[0]), out_...]
where the time goes in v3:
time: 139 us; the launch traced here: 138 us
  Pallas kernels  132 us (95%)
  local copies, waits for them, and re-layouts  5.87 us (4%)
    pallas_call x1, Pallas kernels, on_device(): pl.pallas_call(functools.partial(kernel, ns, nt, nx, taps.shape[0]), out_...  132 us
    unnamed x2, local copies, waits for them, and re-layouts  3.39 us

profile of v3, /device:TPU:2, one launch (start us, length us, event | category | flops | bytes accessed | tf_op | source)
XLA Modules:
  0.0 138.3 jit_solution(3736198426437689209)
XLA Ops:
  0.0 1.2 reshape.11.refs_15_
  1.2 1.3 reshape.9.refs_10_
  2.5 1.6 %copy.17.refs_12_ = f32[2,384,2]{2,1,0:T(8,128)} copy(f32[2,384,2]{1,2,0:T(2,128)} %param.26) | data formatting | bytes 12288 | tf_op args[10]
  4.1 132.4 %shard_map.154 = bf16[96,2048]{1,0:T(8,128)(2,1)} custom-call(bf16[256,256]{1,0:T(8,128)(2,1)} %refs_0_.1, bf16[256,256]{1,0:T(8,128)(2,1)} %refs_1_.1, bf16[256,256]{1,0:T(8,128)(2,1)} %refs_2_.1, bf16[256,256]{1,0:T(8,128)(2,1)} %refs_3_.1, bf16[256,256]{1,0:T(8,128)(2,1)} %refs_4_.1, bf16[256,256]{1,0:T(8,128)(2,1)} %refs_5_.1, bf16[256,256]{1,0:T(8,128)(2,1)} %refs_6_.1, ...), custom_call_target="tpu_custom_call" | custom-call | tf_op jit(solution)/shard_map/pallas_call | solution.py:514
  136.5 1.8 %copy.19 = bf16[96,2048]{1,0:T(8,128)(2,1)} copy(bf16[96,2048]{1,0:T(8,128)(2,1)} %shard_map.154) | data formatting | bytes 786432
